TPU v7x, 32 devices: a whole 2x2x4 slice. The times are simulated.
32 devices in a mesh: fs: 8 (over z, y), tp: 4 (over x, core).
Axes of the slice: x: 2, y: 2, z: 4, core: 2. Of those that a mesh axis runs over, the one named last changes fastest.
Arguments:
- stream: bfloat16 [3072, 2048], P('fs', 'tp'), may hold values from -3 to 3
- gain_first: float32 [2048], replicated, may hold values from 0.1 to 1.9
- gain_mixer: float32 [2048], replicated, may hold values from 0.1 to 1.9
- gain_second: float32 [2048], replicated, may hold values from 0.1 to 1.9
- gate_weight: float32 [2048, 5632], P('fs', 'tp'), may hold values from -0.125 to 0.125
- gate_scale: float32 [5632], P('tp'), may hold values from 0.5 to 2
- up_weight: float32 [2048, 5632], P('fs', 'tp'), may hold values from -0.125 to 0.125
- up_scale: float32 [5632], P('tp'), may hold values from 0.5 to 2
- down_weight: float32 [5632, 2048], P('tp', 'fs'), may hold values from -0.109375 to 0.109375
- down_scale: float32 [2048], P('tp'), may hold values from 0.5 to 2
- pool_in_weight: float32 [2048, 512], P('fs', 'tp'), may hold values from -0.125 to 0.125
- pool_in_scale: float32 [512], P('tp'), may hold values from 0.5 to 2
- pool_out_weight: float32 [512, 2048], P('tp', 'fs'), may hold values from -0.375 to 0.375
- pool_out_scale: float32 [2048], P('tp'), may hold values from 0.5 to 2
Outputs:
- layer_out: bfloat16 [3072, 2048], P('fs', 'tp')
All inputs are finite; a program needn't handle non-finite values.
Results may differ from a plain program's by a relative error of at most 0.025.
Values may be sent and summed in bfloat16 or wider, within the bound.
A program may use at most 64 MiB of HBM per device.

v0:
```python
import jax
import jax.numpy as jnp
from jax import lax
from jax.sharding import PartitionSpec as P

SEQ = 128
eps = 1e-06
WINDOWS = (2, 4, 8, 16)


def normed(own_columns, norm_gain):
    gathered = lax.all_gather(own_columns, "tp", axis=1, tiled=True)
    floats = gathered.astype(jnp.float32)
    scaled = floats * lax.rsqrt(jnp.mean(floats * floats, axis=-1, keepdims=True) + eps)
    return (scaled * norm_gain).astype(jnp.bfloat16)


def residual_add(own_columns, partial_value, column_scale, factor):
    summed = lax.psum_scatter(
        partial_value.astype(jnp.bfloat16), "tp", scatter_dimension=1, tiled=True
    ).astype(jnp.float32)
    return (own_columns.astype(jnp.float32) + factor * (summed * column_scale)).astype(jnp.bfloat16)


def pooling(pool_input):
    channels = pool_input.shape[1]
    floats = pool_input.astype(jnp.float32).reshape(-1, SEQ, channels)
    csum = jnp.concatenate(
        [jnp.zeros((floats.shape[0], 1, channels), jnp.float32), jnp.cumsum(floats, axis=1)], axis=1
    )
    position = jnp.arange(SEQ)
    channel_index = lax.axis_index("tp") * channels + jnp.arange(channels, dtype=jnp.int32)
    channel_group = channel_index * 4 // (channels * lax.axis_size("tp"))
    pooled = -floats
    for group_index, window in enumerate(WINDOWS):
        before = window // 2
        after_span = window - before
        upper_sum = jnp.pad(csum, ((0, 0), (0, after_span), (0, 0)), mode="edge")[
            :, after_span : after_span + SEQ
        ]
        lower_sum = jnp.pad(csum, ((0, 0), (before, 0), (0, 0)), mode="edge")[:, :SEQ]
        counts = (
            jnp.minimum(position + after_span, SEQ) - jnp.maximum(position - before, 0)
        ).astype(jnp.float32)
        window_mean = (upper_sum - lower_sum) / counts[None, :, None]
        select = (channel_group == group_index).astype(jnp.float32)
        pooled = pooled + window_mean * select
    return pooled.reshape(-1, channels).astype(jnp.bfloat16)


def body(
    stream,
    gain_first,
    gain_mixer,
    gain_second,
    gate_weight,
    gate_scale,
    up_weight,
    up_scale,
    down_weight,
    down_scale,
    pool_in_weight,
    pool_in_scale,
    pool_out_weight,
    pool_out_scale,
):
    gate_half = gate_weight.astype(jnp.bfloat16)
    up_half = up_weight.astype(jnp.bfloat16)
    down_half = down_weight.astype(jnp.bfloat16)
    in_half = pool_in_weight.astype(jnp.bfloat16)
    out_half = pool_out_weight.astype(jnp.bfloat16)
    in_whole, out_whole = (
        lax.all_gather(in_half, "fs", axis=0, tiled=True),
        lax.all_gather(out_half, "fs", axis=1, tiled=True),
    )
    gate_whole, up_whole, down_whole = (
        lax.all_gather(gate_half, "fs", axis=0, tiled=True),
        lax.all_gather(up_half, "fs", axis=0, tiled=True),
        lax.all_gather(down_half, "fs", axis=1, tiled=True),
    )

    def feed_forward(normed_rows):
        gate_sum = jnp.dot(normed_rows, gate_whole, preferred_element_type=jnp.float32) * gate_scale
        up_sum = jnp.dot(normed_rows, up_whole, preferred_element_type=jnp.float32) * up_scale
        hidden = (jax.nn.silu(gate_sum) * up_sum).astype(jnp.bfloat16)
        return jnp.dot(hidden, down_whole, preferred_element_type=jnp.float32)

    after_first = residual_add(stream, feed_forward(normed(stream, gain_first)), down_scale, 0.5)
    mixer_normed = normed(after_first, gain_mixer)
    pool_input = (
        jnp.dot(mixer_normed, in_whole, preferred_element_type=jnp.float32) * pool_in_scale
    ).astype(jnp.bfloat16)
    pooled = pooling(pool_input)
    tp_count = lax.axis_size("tp")
    all_pooled = lax.all_gather(pooled, "tp", axis=1, tiled=True)
    out_columns = lax.all_to_all(out_whole, "tp", split_axis=1, concat_axis=0, tiled=True)
    block_width = out_columns.shape[0] // tp_count
    pooled_blocks = all_pooled.reshape(all_pooled.shape[0], tp_count, block_width)
    weight_blocks = out_columns.reshape(tp_count, block_width, out_columns.shape[1])
    partials = jnp.einsum(
        "rbc,bcd->brd", pooled_blocks, weight_blocks, preferred_element_type=jnp.float32
    ).astype(jnp.bfloat16)
    mixed = jnp.sum(partials.astype(jnp.float32), axis=0)
    after_mix = (after_first.astype(jnp.float32) + mixed * pool_out_scale).astype(jnp.bfloat16)
    return residual_add(after_mix, feed_forward(normed(after_mix, gain_second)), down_scale, 0.5)


def solution(mesh):
    placed = (
        P("fs", "tp"),
        P(),
        P(),
        P(),
        P("fs", "tp"),
        P("tp"),
        P("fs", "tp"),
        P("tp"),
        P("tp", "fs"),
        P("tp"),
        P("fs", "tp"),
        P("tp"),
        P("tp", "fs"),
        P("tp"),
    )
    return jax.shard_map(body, mesh=mesh, in_specs=placed, out_specs=P("fs", "tp"), check_vma=False)
```

profile of v0, /device:TPU:0, one launch (start us, length us, event | category | flops | bytes accessed | tf_op | source)
XLA Modules:
  0.0 509.7 jit_solution(2998391872795220859)
XLA Ops:
  6.5 0.0 all-gather.7.cloned.1.call-start
  6.5 0.7 all-gather.7.cloned.1.call-update
  7.3 0.0 all-gather.9.cloned.1.call-start
  7.3 2.3 convert_element_type.144
  9.6 0.0 all-gather.9.cloned.1.call-update
  9.6 0.0 all-gather.11.cloned.1.call-start
  9.7 0.0 copy-done.5
  9.7 1.0 convert_element_type.145
  10.7 0.0 all-gather.11.cloned.1.call-update
  10.7 0.0 copy-start.11
  10.7 0.0 copy-start.13
  10.7 0.0 all-gather.13.cloned.1.call-start
  10.8 0.5 copy-done.6
  11.2 1.0 convert_element_type.147
  12.2 0.0 all-gather.13.cloned.1.call-update
  12.2 0.0 reduce-scatter.3.cloned.1.call-start
  12.3 19.0 %all-gather.7.cloned.1.call-done = bf16[384,2048]{1,0:T(8,128)(2,1)} async-done(((bf16[384,512]{1,0:T(8,128)(2,1)}), bf16[384,2048]{1,0:T(8,128)(2,1)}) %all-gather.7.cloned.1.call-update) | async-done | bytes 1572880 | tf_op jit(solution)/shard_map/all_gather | solution.py:12
  31.3 1.8 fusion
  33.1 0.0 copy-start.14
  33.1 92.7 %all-gather.9.cloned.1.call-done = bf16[2048,1408]{1,0:T(8,128)(2,1)} async-done(((bf16[256,1408]{1,0:T(8,128)(2,1)}), bf16[2048,1408]{1,0:T(8,128)(2,1)}) %all-gather.9.cloned.1.call-update) | async-done | bytes 5767184 | tf_op jit(solution)/shard_map/all_gather | solution.py:77
  125.8 0.0 copy-done.11
  125.8 0.0 copy-done.13
  125.8 7.1 %convolution_multiply_fusion.3 = f32[384,1408]{1,0:T(8,128)} fusion(bf16[2048,1408]{1,0:T(8,128)(2,1)} %all-gather.9.cloned.1.call-done, f32[1408]{0:T(1024)S(1)} %copy-done.13, bf16[384,2048]{1,0:T(8,128)(2,1)} %all-gather.7.cloned.1.call-done, f32[2048]{0:T(1024)S(1)} %copy-done.11, f32[384]{0:T(512)S(1)} %add_rsqrt_fusion.2), kind=kOutput, calls=%fused_computation.21 | convolution fusion | flops 2218278912 | bytes 9518080 | tf_op jit(solution)/shard_map/dot_general | solution.py:83
  133.0 85.6 %all-gather.11.cloned.1.call-done = bf16[2048,1408]{1,0:T(8,128)(2,1)} async-done(((bf16[256,1408]{1,0:T(8,128)(2,1)}), bf16[2048,1408]{1,0:T(8,128)(2,1)}) %all-gather.11.cloned.1.call-update) | async-done | bytes 5767184 | tf_op jit(solution)/shard_map/all_gather | solution.py:78
  218.5 93.2 %all-gather.13.cloned.1.call-done = bf16[1408,2048]{1,0:T(8,128)(2,1)} async-done(((bf16[1408,256]{1,0:T(8,128)(2,1)}), bf16[1408,2048]{1,0:T(8,128)(2,1)}) %all-gather.13.cloned.1.call-update) | async-done | bytes 5767184 | tf_op jit(solution)/shard_map/all_gather | solution.py:79
  311.8 0.0 copy-done.2
  311.8 0.0 copy-done.14
  311.8 11.2 %convolution_convert_fusion.1 = bf16[384,2048]{1,0:T(8,128)(2,1)} fusion(bf16[1408,2048]{1,0:T(8,128)(2,1)} %all-gather.13.cloned.1.call-done, bf16[2048,1408]{1,0:T(8,128)(2,1)} %all-gather.11.cloned.1.call-done, f32[384,1408]{1,0:T(8,128)} %convolution_multiply_fusion.3, f32[1408]{0:T(1024)S(1)} %copy-done.14, bf16[384,2048]{1,0:T(8,128)(2,1)S(1)} %copy-done.2, ...), kind=kOutput, calls=%fused_computation.23 | convolution fusion | flops 4436901888 | bytes 16858112 | tf_op jit(solution)/shard_map/dot_general | solution.py:86
  323.0 0.0 reduce-scatter.3.cloned.1.call-update
  323.0 0.0 copy-start.8
  323.0 0.0 all-gather.15.cloned.1.call-start
  323.1 26.3 %reduce-scatter.3.cloned.1.call-done = bf16[384,512]{1,0:T(8,128)(2,1)} async-done(((bf16[384,2048]{1,0:T(8,128)(2,1)}), bf16[384,512]{1,0:T(8,128)(2,1)}) %reduce-scatter.3.cloned.1.call-update) | async-done | bytes 393232 | tf_op jit(solution)/shard_map/reduce_scatter | solution.py:19
  349.3 0.0 copy-done.4
  349.3 1.9 add_convert_fusion.2
  351.2 0.0 all-gather.15.cloned.1.call-update
  351.3 0.1 copy.16
  351.4 31.7 %all_gather.34 = bf16[128,2048]{0,1:T(8,128)(2,1)S(1)} all-gather(bf16[128,256]{0,1:T(8,128)(2,1)S(1)} %copy.16), channel_id=1, replica_groups=mesh['fs'=8,'tp'=4] {'fs'}, dimensions={1}, use_global_device_ids=true | all-gather | bytes 589824 | tf_op jit(solution)/shard_map/all_gather | solution.py:74
  383.1 1.0 copy.17
  384.1 3.5 all-to-all-start
  387.6 0.0 all-gather.17.cloned.1.call-start
  387.8 31.5 %all_gather.32 = bf16[2048,128]{1,0:T(8,128)(2,1)S(1)} all-gather(bf16[256,128]{1,0:T(8,128)(2,1)S(1)} %convert_element_type.154), channel_id=1, replica_groups=mesh['fs'=8,'tp'=4] {'fs'}, dimensions={0}, use_global_device_ids=true | all-gather | bytes 589824 | tf_op jit(solution)/shard_map/all_gather | solution.py:73
  419.3 1.8 fusion.3
  421.1 0.0 copy-done.12
  421.1 2.0 fusion.20
  423.2 0.0 copy-start
  423.2 0.0 copy-start.10
  423.2 0.2 reduce_window_sum.11
  423.5 0.3 fusion.46
  423.8 0.1 copy.15
  423.9 6.7 %all_gather.33 = bf16[384,512]{0,1:T(8,128)(2,1)S(1)} all-gather(bf16[384,128]{0,1:T(8,128)(2,1)S(1)} %copy.15), channel_id=1, replica_groups=mesh['fs'=8,'tp'=4] {'tp'}, dimensions={1}, use_global_device_ids=true | all-gather | bytes 491520 | tf_op jit(solution)/shard_map/all_gather | solution.py:95
  430.6 0.0 all-to-all-done
  430.6 0.6 convert_reduce_fusion
  431.2 0.0 copy-start.15
  431.2 0.9 add_convert_fusion.1
  432.1 0.0 all-gather.17.cloned.1.call-update
  432.1 0.2 reduce-scatter.5.cloned.1.call-start
  432.4 20.1 %all-gather.17.cloned.1.call-done = bf16[384,2048]{1,0:T(8,128)(2,1)} async-done(((bf16[384,512]{1,0:T(8,128)(2,1)}), bf16[384,2048]{1,0:T(8,128)(2,1)}) %all-gather.17.cloned.1.call-update) | async-done | bytes 1572880 | tf_op jit(solution)/shard_map/all_gather | solution.py:12
  452.4 1.8 fusion.6
  454.3 7.2 %convolution_multiply_fusion.1 = f32[384,1408]{1,0:T(8,128)} fusion(bf16[2048,1408]{1,0:T(8,128)(2,1)} %all-gather.9.cloned.1.call-done, f32[1408]{0:T(1024)S(1)} %copy-done.13, bf16[384,2048]{1,0:T(8,128)(2,1)} %all-gather.17.cloned.1.call-done, f32[2048]{0:T(1024)S(1)} %copy-done.15, f32[384]{0:T(512)S(1)} %add_rsqrt_fusion), kind=kOutput, calls=%fused_computation.18 | convolution fusion | flops 2218278912 | bytes 9518080 | tf_op jit(solution)/shard_map/dot_general | solution.py:83
  461.5 11.3 %convolution_convert_fusion = bf16[384,2048]{1,0:T(8,128)(2,1)} fusion(bf16[1408,2048]{1,0:T(8,128)(2,1)} %all-gather.13.cloned.1.call-done, bf16[2048,1408]{1,0:T(8,128)(2,1)} %all-gather.11.cloned.1.call-done, f32[384,1408]{1,0:T(8,128)} %convolution_multiply_fusion.1, f32[1408]{0:T(1024)S(1)} %copy-done.14, bf16[384,2048]{1,0:T(8,128)(2,1)S(1)} %copy-done.3, ...), kind=kOutput, calls=%fused_computation.22 | convolution fusion | flops 4436901888 | bytes 16858112 | tf_op jit(solution)/shard_map/dot_general | solution.py:86
  472.8 0.0 reduce-scatter.5.cloned.1.call-update
  472.8 28.1 %reduce-scatter.5.cloned.1.call-done = bf16[384,512]{1,0:T(8,128)(2,1)} async-done(((bf16[384,2048]{1,0:T(8,128)(2,1)}), bf16[384,512]{1,0:T(8,128)(2,1)}) %reduce-scatter.5.cloned.1.call-update) | async-done | bytes 393232 | tf_op jit(solution)/shard_map/reduce_scatter | solution.py:19
  501.0 0.0 copy-done.1
  501.0 1.9 add_convert_fusion
  (38 shorter events, 0.2 us)
Async XLA Ops:
  6.5 3.2 copy-start.5
  6.5 24.7 %all-gather.7.cloned.1.call-start = ((), (), s32[]{:S(2)}) async-start(), calls=%async_computation.3 | async-start | bytes 1966080 | tf_op jit(solution)/shard_map/all_gather | solution.py:12
  7.3 118.5 %all-gather.9.cloned.1.call-start = ((), (), s32[]{:S(2)}) async-start(), calls=%async_computation.4 | async-start | bytes 6488064 | tf_op jit(solution)/shard_map/all_gather | solution.py:77
  9.6 1.6 copy-start.6
  9.6 208.9 %all-gather.11.cloned.1.call-start = ((), (), s32[]{:S(2)}) async-start(), calls=%async_computation.5 | async-start | bytes 6488064 | tf_op jit(solution)/shard_map/all_gather | solution.py:78
  10.7 115.1 %copy-start.11 = (f32[2048]{0:T(1024)S(1)}, f32[2048]{0:T(1024)}, u32[]{:S(2)}) copy-start(f32[2048]{0:T(1024)} %param.15) | copy-start | bytes 24580
  10.7 115.1 %copy-start.13 = (f32[1408]{0:T(1024)S(1)}, f32[1408]{0:T(1024)}, u32[]{:S(2)}) copy-start(f32[1408]{0:T(1024)} %param.19) | copy-start | bytes 16900
  10.7 301.1 %all-gather.13.cloned.1.call-start = ((), (), s32[]{:S(2)}) async-start(), calls=%async_computation.6 | async-start | bytes 6488064 | tf_op jit(solution)/shard_map/all_gather | solution.py:79
  12.2 337.1 %reduce-scatter.3.cloned.1.call-start = ((), (), s32[]{:S(2)}) async-start(), calls=%async_computation.7 | async-start | bytes 1966080 | tf_op jit(solution)/shard_map/reduce_scatter | solution.py:19
  33.1 278.7 %copy-start.2 = (bf16[384,2048]{1,0:T(8,128)(2,1)S(1)}, bf16[384,2048]{1,0:T(8,128)(2,1)}, u32[]{:S(2)}) copy-start(bf16[384,2048]{1,0:T(8,128)(2,1)} %all-gather.7.cloned.1.call-done) | copy-start | bytes 4718596
  33.1 278.7 %copy-start.14 = (f32[1408]{0:T(1024)S(1)}, f32[1408]{0:T(1024)}, u32[]{:S(2)}) copy-start(f32[1408]{0:T(1024)} %param.21) | copy-start | bytes 16900
  133.0 216.4 %copy-start.4 = (bf16[384,512]{1,0:T(8,128)(2,1)S(1)}, bf16[384,512]{1,0:T(8,128)(2,1)}, u32[]{:S(2)}) copy-start(bf16[384,512]{1,0:T(8,128)(2,1)} %param.14) | copy-start | bytes 1179652
  133.0 216.4 %copy-start.9 = (f32[512]{0:T(512)S(1)}, f32[512]{0:T(512)}, u32[]{:S(2)}) copy-start(f32[512]{0:T(512)} %param.23) | copy-start | bytes 6148
  323.0 28.3 %copy-start.7 = (f32[128,256]{1,0:T(8,128)S(1)}, f32[128,256]{1,0:T(8,128)}, u32[]{:S(2)}) copy-start(f32[128,256]{1,0:T(8,128)} %param.26) | copy-start | bytes 393220
  323.0 64.6 %copy-start.8 = (f32[256,128]{1,0:T(8,128)S(1)}, f32[256,128]{1,0:T(8,128)}, u32[]{:S(2)}) copy-start(f32[256,128]{1,0:T(8,128)} %param.24) | copy-start | bytes 393220
  323.0 96.3 %all-gather.15.cloned.1.call-start = ((), (), s32[]{:S(2)}) async-start(), calls=%async_computation.8 | async-start | bytes 1966080 | tf_op jit(solution)/shard_map/all_gather | solution.py:12
  383.1 38.0 %copy-start.12 = (f32[2048]{0:T(1024)S(1)}, f32[2048]{0:T(1024)}, u32[]{:S(2)}) copy-start(f32[2048]{0:T(1024)} %param.16) | copy-start | bytes 24580
  383.1 38.0 %copy-start.16 = (f32[128]{0:T(128)S(1)}, f32[128]{0:T(128)}, u32[]{:S(2)}) copy-start(f32[128]{0:T(128)} %param.25) | copy-start | bytes 1540
  384.1 46.5 %all-to-all-start = ((bf16[128,4,512]{2,0,1:T(8,128)(2,1)}), bf16[128,4,512]{2,0,1:T(8,128)(2,1)S(1)}, u32[]{:S(2)}, u32[]{:S(2)}) async-start(bf16[128,4,512]{2,0,1:T(8,128)(2,1)} %copy.17), calls=%async_computation.1 | async-start | bytes 1048576 | tf_op jit(solution)/shard_map/all_to_all | solution.py:96
  387.6 64.9 %all-gather.17.cloned.1.call-start = ((), (), s32[]{:S(2)}) async-start(), calls=%async_computation.9 | async-start | bytes 1966080 | tf_op jit(solution)/shard_map/all_gather | solution.py:12
  423.2 8.0 %copy-start = (bf16[384,512]{1,0:T(8,128)(2,1)S(1)}, bf16[384,512]{1,0:T(8,128)(2,1)}, u32[]{:S(2)}) copy-start(bf16[384,512]{1,0:T(8,128)(2,1)} %add_convert_fusion.2) | copy-start | bytes 1179652
  423.2 8.0 %copy-start.10 = (f32[512]{0:T(512)S(1)}, f32[512]{0:T(512)}, u32[]{:S(2)}) copy-start(f32[512]{0:T(512)} %param.27) | copy-start | bytes 6148
  431.2 23.0 %copy-start.15 = (f32[2048]{0:T(1024)S(1)}, f32[2048]{0:T(1024)}, u32[]{:S(2)}) copy-start(f32[2048]{0:T(1024)} %param.17) | copy-start | bytes 24580
  432.1 68.8 %reduce-scatter.5.cloned.1.call-start = ((), (), s32[]{:S(2)}) async-start(), calls=%async_computation.10 | async-start | bytes 1966080 | tf_op jit(solution)/shard_map/reduce_scatter | solution.py:19
  454.3 7.3 %copy-start.3 = (bf16[384,2048]{1,0:T(8,128)(2,1)S(1)}, bf16[384,2048]{1,0:T(8,128)(2,1)}, u32[]{:S(2)}) copy-start(bf16[384,2048]{1,0:T(8,128)(2,1)} %all-gather.17.cloned.1.call-done) | copy-start | bytes 4718596
  461.5 39.4 %copy-start.1 = (bf16[384,512]{1,0:T(8,128)(2,1)S(1)}, bf16[384,512]{1,0:T(8,128)(2,1)}, u32[]{:S(2)}) copy-start(bf16[384,512]{1,0:T(8,128)(2,1)} %add_convert_fusion.1) | copy-start | bytes 1179652
Sparse Core Ops, SparseCore 0:
  8.9 22.3 all-gather.6
  33.5 92.2 all-gather.8
  128.0 90.4 all-gather.10
  220.4 91.2 all-gather.12
  323.1 26.1 reduce-scatter.2
  351.4 19.6 all-gather.14
  432.3 20.1 all-gather.16
  472.9 27.9 reduce-scatter.4
where the time goes:
time: 510 us
  waiting for transfers between devices  366 us (72%)
  blocking collectives  69.9 us (14%)
  matrix products  39.5 us (8%)
  other arithmetic  14.9 us (3%)
  between operations  13.8 us (3%)
    all_gather x1, waiting for transfers between devices, body(): lax.all_gather(down_half, 'fs', axis=1, tiled=True)  93.2 us
    all_gather x1, waiting for transfers between devices, body(): lax.all_gather(gate_half, 'fs', axis=0, tiled=True)  92.7 us
    all_gather x1, waiting for transfers between devices, body(): lax.all_gather(up_half, 'fs', axis=0, tiled=True)  85.6 us
    reduce_scatter x2, waiting for transfers between devices, residual_add(): lax.psum_scatter(partial_value.astype(jnp.bfloat16), 'tp', scatter_dimens...  54.4 us
    all_gather x3, waiting for transfers between devices, normed(): gathered = lax.all_gather(own_columns, 'tp', axis=1, tiled=True)  39.1 us
    all_gather x1, blocking collectives, body(): lax.all_gather(out_half, 'fs', axis=1, tiled=True)  31.7 us
    all_gather x1, blocking collectives, body(): lax.all_gather(in_half, 'fs', axis=0, tiled=True)  31.5 us
    dot_general x2, matrix products, feed_forward(): return jnp.dot(hidden, down_whole, preferred_element_type=jnp.float32)  22.5 us
  transfers between devices with their start and end apart: 9, of which 7 were waited for; matrix products, arithmetic and copies ran while one was open for 4% of the time, Pallas kernels for 0%

commit v1 on v0

--- a/solution.py
+++ b/solution.py
@@ -76,7 +76,7 @@
     gate_whole, up_whole, down_whole = (
         lax.all_gather(gate_half, "fs", axis=0, tiled=True),
         lax.all_gather(up_half, "fs", axis=0, tiled=True),
-        lax.all_gather(down_half, "fs", axis=1, tiled=True),
+        jnp.concatenate(lax.all_gather(down_half, "fs"), axis=1),
     )
 
     def feed_forward(normed_rows):

time: 510 us -> 510 us (level)
  waiting for transfers between devices: 366 us -> 357 us
  local copies, waits for them, and re-layouts: 1.86 us -> 10.1 us
    all_gather x1, waiting for transfers between devices: 92.7 us -> 84.4 us  [body(): lax.all_gather(gate_half, 'fs', axis=0, tiled=True)]
    reshape x0 -> x1, local copies, waits for them, and re-layouts: none -> 8.3 us  [body(): jnp.concatenate(lax.all_gather(down_half, 'fs'), axis=1)]
  transfers between devices with their start and end apart: 9 -> 9, of which waited for: 7 -> 7; matrix products, arithmetic and copies ran while one was open for 4% -> 5% of each run, Pallas kernels for 0% -> 0%
where the time goes in v1:
time: 510 us; the launch traced here: 509 us
  waiting for transfers between devices  357 us (70%)
  blocking collectives  69.9 us (14%)
  matrix products  39 us (8%)
  other arithmetic  14.9 us (3%)
  between operations  13.8 us (3%)
  local copies, waits for them, and re-layouts  10.1 us (2%)
    all_gather x1, waiting for transfers between devices, body(): lax.all_gather(down_half, 'fs')  92.7 us
    all_gather x1, waiting for transfers between devices, body(): lax.all_gather(up_half, 'fs', axis=0, tiled=True)  85.9 us
    all_gather x1, waiting for transfers between devices, body(): lax.all_gather(gate_half, 'fs', axis=0, tiled=True)  84.4 us
    reduce_scatter x2, waiting for transfers between devices, residual_add(): lax.psum_scatter(partial_value.astype(jnp.bfloat16), 'tp', scatter_dimens...  54.4 us
    all_gather x3, waiting for transfers between devices, normed(): gathered = lax.all_gather(own_columns, 'tp', axis=1, tiled=True)  39.1 us
    all_gather x1, blocking collectives, body(): lax.all_gather(out_half, 'fs', axis=1, tiled=True)  31.7 us
    all_gather x1, blocking collectives, body(): lax.all_gather(in_half, 'fs', axis=0, tiled=True)  31.5 us
    dot_general x2, matrix products, feed_forward(): return jnp.dot(hidden, down_whole, preferred_element_type=jnp.float32)  22.5 us
  transfers between devices with their start and end apart: 9, of which 7 were waited for; matrix products, arithmetic and copies ran while one was open for 5% of the time, Pallas kernels for 0%

profile of v1, /device:TPU:0, one launch (start us, length us, event | category | flops | bytes accessed | tf_op | source)
XLA Modules:
  0.0 509.0 jit_solution(758110273829904852)
XLA Ops:
  6.5 0.0 all-gather.8.cloned.1.call-start
  6.5 0.7 all-gather.8.cloned.1.call-update
  7.3 0.0 all-gather.18.cloned.1.call-start
  7.3 2.3 convert_element_type.147
  9.6 0.0 all-gather.18.cloned.1.call-update
  9.6 0.0 all-gather.10.cloned.1.call-start
  9.7 0.0 copy-done.5
  9.7 1.0 convert_element_type.144
  10.7 0.0 all-gather.10.cloned.1.call-update
  10.7 0.0 all-gather.12.cloned.1.call-start
  10.8 0.5 copy-done.6
  11.2 1.0 convert_element_type.145
  12.2 0.0 all-gather.12.cloned.1.call-update
  12.3 0.0 reduce-scatter.3.cloned.1.call-start
  12.3 19.0 %all-gather.8.cloned.1.call-done = bf16[384,2048]{1,0:T(8,128)(2,1)} async-done(((bf16[384,512]{1,0:T(8,128)(2,1)}), bf16[384,2048]{1,0:T(8,128)(2,1)}) %all-gather.8.cloned.1.call-update) | async-done | bytes 1572880 | tf_op jit(solution)/shard_map/all_gather | solution.py:12
  31.3 1.8 fusion
  33.1 92.7 %all-gather.18.cloned.1.call-done = bf16[11264,256]{1,0:T(8,128)(2,1)} async-done(((bf16[1408,256]{1,0:T(8,128)(2,1)}), bf16[11264,256]{1,0:T(8,128)(2,1)}) %all-gather.18.cloned.1.call-update) | async-done | bytes 5767184 | tf_op jit(solution)/shard_map/all_gather | solution.py:79
  125.8 8.3 %copy.19 = bf16[1408,8,256]{0,2,1:T(8,128)(2,1)} copy(bf16[1408,8,256]{2,0,1:T(8,128)(2,1)} %bitcast.25) | data formatting | bytes 11534336 | tf_op jit(solution)/shard_map/reshape | solution.py:79
  134.1 84.4 %all-gather.10.cloned.1.call-done = bf16[2048,1408]{1,0:T(8,128)(2,1)} async-done(((bf16[256,1408]{1,0:T(8,128)(2,1)}), bf16[2048,1408]{1,0:T(8,128)(2,1)}) %all-gather.10.cloned.1.call-update) | async-done | bytes 5767184 | tf_op jit(solution)/shard_map/all_gather | solution.py:77
  218.5 0.0 copy-done.2
  218.5 0.0 copy-done.11
  218.5 6.7 %convolution_multiply_fusion.3 = f32[384,1408]{1,0:T(8,128)} fusion(bf16[2048,1408]{1,0:T(8,128)(2,1)} %all-gather.10.cloned.1.call-done, f32[1408]{0:T(1024)S(1)} %copy-done.13, bf16[384,2048]{1,0:T(8,128)(2,1)S(1)} %copy-done.2, f32[2048]{0:T(1024)S(1)} %copy-done.11, f32[384]{0:T(512)S(1)} %add_rsqrt_fusion.2), kind=kOutput, calls=%fused_computation.21 | convolution fusion | flops 2218278912 | bytes 9518080 | tf_op jit(solution)/shard_map/dot_general | solution.py:83
  225.2 85.9 %all-gather.12.cloned.1.call-done = bf16[2048,1408]{1,0:T(8,128)(2,1)} async-done(((bf16[256,1408]{1,0:T(8,128)(2,1)}), bf16[2048,1408]{1,0:T(8,128)(2,1)}) %all-gather.12.cloned.1.call-update) | async-done | bytes 5767184 | tf_op jit(solution)/shard_map/all_gather | solution.py:78
  311.1 11.3 %convolution_convert_fusion.1 = bf16[384,2048]{1,0:T(8,128)(2,1)} fusion(bf16[1408,2048]{0,1:T(8,128)(2,1)} %bitcast.23, bf16[2048,1408]{1,0:T(8,128)(2,1)} %all-gather.12.cloned.1.call-done, f32[384,1408]{1,0:T(8,128)} %convolution_multiply_fusion.3, f32[1408]{0:T(1024)S(1)} %copy-done.14, bf16[384,2048]{1,0:T(8,128)(2,1)S(1)} %copy-done.2, ...), kind=kOutput, calls=%fused_computation.23 | convolution fusion | flops 4436901888 | bytes 16858112 | tf_op jit(solution)/shard_map/dot_general | solution.py:86
  322.3 0.0 reduce-scatter.3.cloned.1.call-update
  322.4 0.0 copy-start.8
  322.4 0.0 all-gather.14.cloned.1.call-start
  322.4 26.3 %reduce-scatter.3.cloned.1.call-done = bf16[384,512]{1,0:T(8,128)(2,1)} async-done(((bf16[384,2048]{1,0:T(8,128)(2,1)}), bf16[384,512]{1,0:T(8,128)(2,1)}) %reduce-scatter.3.cloned.1.call-update) | async-done | bytes 393232 | tf_op jit(solution)/shard_map/reduce_scatter | solution.py:19
  348.7 0.0 copy-done.4
  348.7 1.9 add_convert_fusion.2
  350.6 0.0 all-gather.14.cloned.1.call-update
  350.6 0.0 copy-done.7
  350.6 0.1 copy.21
  350.7 31.7 %all_gather.38 = bf16[128,2048]{0,1:T(8,128)(2,1)S(1)} all-gather(bf16[128,256]{0,1:T(8,128)(2,1)S(1)} %copy.21), channel_id=1, replica_groups=mesh['fs'=8,'tp'=4] {'fs'}, dimensions={1}, use_global_device_ids=true | all-gather | bytes 589824 | tf_op jit(solution)/shard_map/all_gather | solution.py:74
  382.5 1.0 copy.22
  383.5 3.5 all-to-all-start
  387.0 0.0 all-gather.16.cloned.1.call-start
  387.2 31.5 %all_gather.36 = bf16[2048,128]{1,0:T(8,128)(2,1)S(1)} all-gather(bf16[256,128]{1,0:T(8,128)(2,1)S(1)} %convert_element_type.154), channel_id=1, replica_groups=mesh['fs'=8,'tp'=4] {'fs'}, dimensions={0}, use_global_device_ids=true | all-gather | bytes 589824 | tf_op jit(solution)/shard_map/all_gather | solution.py:73
  418.7 1.8 fusion.3
  420.5 0.0 copy-done.12
  420.5 2.0 fusion.20
  422.5 0.0 copy-start
  422.5 0.0 copy-start.10
  422.6 0.2 reduce_window_sum.11
  422.8 0.3 fusion.46
  423.1 0.1 copy.20
  423.3 6.7 %all_gather.37 = bf16[384,512]{0,1:T(8,128)(2,1)S(1)} all-gather(bf16[384,128]{0,1:T(8,128)(2,1)S(1)} %copy.20), channel_id=1, replica_groups=mesh['fs'=8,'tp'=4] {'tp'}, dimensions={1}, use_global_device_ids=true | all-gather | bytes 491520 | tf_op jit(solution)/shard_map/all_gather | solution.py:95
  429.9 0.0 all-to-all-done
  429.9 0.6 convert_reduce_fusion
  430.5 0.0 copy-done
  430.6 0.0 copy-done.10
  430.6 0.0 copy-start.15
  430.6 0.9 add_convert_fusion.1
  431.5 0.0 all-gather.16.cloned.1.call-update
  431.5 0.2 reduce-scatter.5.cloned.1.call-start
  431.7 20.1 %all-gather.16.cloned.1.call-done = bf16[384,2048]{1,0:T(8,128)(2,1)} async-done(((bf16[384,512]{1,0:T(8,128)(2,1)}), bf16[384,2048]{1,0:T(8,128)(2,1)}) %all-gather.16.cloned.1.call-update) | async-done | bytes 1572880 | tf_op jit(solution)/shard_map/all_gather | solution.py:12
  451.8 1.8 fusion.6
  453.6 0.0 copy-done.15
  453.6 0.0 copy-start.3
  453.6 7.2 %convolution_multiply_fusion.1 = f32[384,1408]{1,0:T(8,128)} fusion(bf16[2048,1408]{1,0:T(8,128)(2,1)} %all-gather.10.cloned.1.call-done, f32[1408]{0:T(1024)S(1)} %copy-done.13, bf16[384,2048]{1,0:T(8,128)(2,1)} %all-gather.16.cloned.1.call-done, f32[2048]{0:T(1024)S(1)} %copy-done.15, f32[384]{0:T(512)S(1)} %add_rsqrt_fusion), kind=kOutput, calls=%fused_computation.18 | convolution fusion | flops 2218278912 | bytes 9518080 | tf_op jit(solution)/shard_map/dot_general | solution.py:83
  460.9 11.3 %convolution_convert_fusion = bf16[384,2048]{1,0:T(8,128)(2,1)} fusion(bf16[1408,2048]{0,1:T(8,128)(2,1)} %bitcast.24, bf16[2048,1408]{1,0:T(8,128)(2,1)} %all-gather.12.cloned.1.call-done, f32[384,1408]{1,0:T(8,128)} %convolution_multiply_fusion.1, f32[1408]{0:T(1024)S(1)} %copy-done.14, bf16[384,2048]{1,0:T(8,128)(2,1)S(1)} %copy-done.3, ...), kind=kOutput, calls=%fused_computation.22 | convolution fusion | flops 4436901888 | bytes 16858112 | tf_op jit(solution)/shard_map/dot_general | solution.py:86
  472.1 0.0 reduce-scatter.5.cloned.1.call-update
  472.2 28.2 %reduce-scatter.5.cloned.1.call-done = bf16[384,512]{1,0:T(8,128)(2,1)} async-done(((bf16[384,2048]{1,0:T(8,128)(2,1)}), bf16[384,512]{1,0:T(8,128)(2,1)}) %reduce-scatter.5.cloned.1.call-update) | async-done | bytes 393232 | tf_op jit(solution)/shard_map/reduce_scatter | solution.py:19
  500.3 1.9 add_convert_fusion
  (39 shorter events, 0.2 us)
Async XLA Ops:
  6.5 3.2 copy-start.5
  6.5 24.7 %all-gather.8.cloned.1.call-start = ((), (), s32[]{:S(2)}) async-start(), calls=%async_computation.3 | async-start | bytes 1966080 | tf_op jit(solution)/shard_map/all_gather | solution.py:12
  7.3 118.5 %all-gather.18.cloned.1.call-start = ((), (), s32[]{:S(2)}) async-start(), calls=%async_computation.10 | async-start | bytes 6488064 | tf_op jit(solution)/shard_map/all_gather | solution.py:79
  9.6 1.6 copy-start.6
  9.6 208.9 %all-gather.10.cloned.1.call-start = ((), (), s32[]{:S(2)}) async-start(), calls=%async_computation.4 | async-start | bytes 6488064 | tf_op jit(solution)/shard_map/all_gather | solution.py:77
  10.7 300.4 %all-gather.12.cloned.1.call-start = ((), (), s32[]{:S(2)}) async-start(), calls=%async_computation.5 | async-start | bytes 6488064 | tf_op jit(solution)/shard_map/all_gather | solution.py:78
  12.3 336.4 %reduce-scatter.3.cloned.1.call-start = ((), (), s32[]{:S(2)}) async-start(), calls=%async_computation.6 | async-start | bytes 1966080 | tf_op jit(solution)/shard_map/reduce_scatter | solution.py:19
  125.8 92.7 %copy-start.2 = (bf16[384,2048]{1,0:T(8,128)(2,1)S(1)}, bf16[384,2048]{1,0:T(8,128)(2,1)}, u32[]{:S(2)}) copy-start(bf16[384,2048]{1,0:T(8,128)(2,1)} %all-gather.8.cloned.1.call-done) | copy-start | bytes 4718596
  125.8 92.7 %copy-start.11 = (f32[2048]{0:T(1024)S(1)}, f32[2048]{0:T(1024)}, u32[]{:S(2)}) copy-start(f32[2048]{0:T(1024)} %param.15) | copy-start | bytes 24580
  125.8 92.7 %copy-start.13 = (f32[1408]{0:T(1024)S(1)}, f32[1408]{0:T(1024)}, u32[]{:S(2)}) copy-start(f32[1408]{0:T(1024)} %param.19) | copy-start | bytes 16900
  134.1 177.0 %copy-start.14 = (f32[1408]{0:T(1024)S(1)}, f32[1408]{0:T(1024)}, u32[]{:S(2)}) copy-start(f32[1408]{0:T(1024)} %param.21) | copy-start | bytes 16900
  311.1 37.6 %copy-start.4 = (bf16[384,512]{1,0:T(8,128)(2,1)S(1)}, bf16[384,512]{1,0:T(8,128)(2,1)}, u32[]{:S(2)}) copy-start(bf16[384,512]{1,0:T(8,128)(2,1)} %param.14) | copy-start | bytes 1179652
  311.1 37.6 %copy-start.9 = (f32[512]{0:T(512)S(1)}, f32[512]{0:T(512)}, u32[]{:S(2)}) copy-start(f32[512]{0:T(512)} %param.23) | copy-start | bytes 6148
  322.3 28.3 %copy-start.7 = (f32[128,256]{1,0:T(8,128)S(1)}, f32[128,256]{1,0:T(8,128)}, u32[]{:S(2)}) copy-start(f32[128,256]{1,0:T(8,128)} %param.26) | copy-start | bytes 393220
  322.4 64.7 %copy-start.8 = (f32[256,128]{1,0:T(8,128)S(1)}, f32[256,128]{1,0:T(8,128)}, u32[]{:S(2)}) copy-start(f32[256,128]{1,0:T(8,128)} %param.24) | copy-start | bytes 393220
  322.4 96.3 %all-gather.14.cloned.1.call-start = ((), (), s32[]{:S(2)}) async-start(), calls=%async_computation.7 | async-start | bytes 1966080 | tf_op jit(solution)/shard_map/all_gather | solution.py:12
  382.5 38.0 %copy-start.12 = (f32[2048]{0:T(1024)S(1)}, f32[2048]{0:T(1024)}, u32[]{:S(2)}) copy-start(f32[2048]{0:T(1024)} %param.16) | copy-start | bytes 24580
  382.5 38.0 %copy-start.16 = (f32[128]{0:T(128)S(1)}, f32[128]{0:T(128)}, u32[]{:S(2)}) copy-start(f32[128]{0:T(128)} %param.25) | copy-start | bytes 1540
  383.5 46.4 %all-to-all-start = ((bf16[128,4,512]{2,0,1:T(8,128)(2,1)}), bf16[128,4,512]{2,0,1:T(8,128)(2,1)S(1)}, u32[]{:S(2)}, u32[]{:S(2)}) async-start(bf16[128,4,512]{2,0,1:T(8,128)(2,1)} %copy.22), calls=%async_computation.1 | async-start | bytes 1048576 | tf_op jit(solution)/shard_map/all_to_all | solution.py:96
  387.0 64.9 %all-gather.16.cloned.1.call-start = ((), (), s32[]{:S(2)}) async-start(), calls=%async_computation.8 | async-start | bytes 1966080 | tf_op jit(solution)/shard_map/all_gather | solution.py:12
  422.5 8.0 %copy-start = (bf16[384,512]{1,0:T(8,128)(2,1)S(1)}, bf16[384,512]{1,0:T(8,128)(2,1)}, u32[]{:S(2)}) copy-start(bf16[384,512]{1,0:T(8,128)(2,1)} %add_convert_fusion.2) | copy-start | bytes 1179652
  422.5 8.0 %copy-start.10 = (f32[512]{0:T(512)S(1)}, f32[512]{0:T(512)}, u32[]{:S(2)}) copy-start(f32[512]{0:T(512)} %param.27) | copy-start | bytes 6148
  430.6 23.1 %copy-start.15 = (f32[2048]{0:T(1024)S(1)}, f32[2048]{0:T(1024)}, u32[]{:S(2)}) copy-start(f32[2048]{0:T(1024)} %param.17) | copy-start | bytes 24580
  431.5 68.8 %reduce-scatter.5.cloned.1.call-start = ((), (), s32[]{:S(2)}) async-start(), calls=%async_computation.9 | async-start | bytes 1966080 | tf_op jit(solution)/shard_map/reduce_scatter | solution.py:19
  453.6 7.3 %copy-start.3 = (bf16[384,2048]{1,0:T(8,128)(2,1)S(1)}, bf16[384,2048]{1,0:T(8,128)(2,1)}, u32[]{:S(2)}) copy-start(bf16[384,2048]{1,0:T(8,128)(2,1)} %all-gather.16.cloned.1.call-done) | copy-start | bytes 4718596
  460.9 39.4 %copy-start.1 = (bf16[384,512]{1,0:T(8,128)(2,1)S(1)}, bf16[384,512]{1,0:T(8,128)(2,1)}, u32[]{:S(2)}) copy-start(bf16[384,512]{1,0:T(8,128)(2,1)} %add_convert_fusion.1) | copy-start | bytes 1179652
Sparse Core Ops, SparseCore 0:
  8.9 22.3 all-gather.7
  33.5 92.2 all-gather.17
  128.0 90.4 all-gather.9
  220.6 90.4 all-gather.11
  322.5 26.1 reduce-scatter.2
  350.7 19.6 all-gather.13
  431.6 20.1 all-gather.15
  472.3 27.9 reduce-scatter.4
